TPU v7x, 32 devices: a whole 2x2x4 slice. The times are simulated.
32 devices in a mesh: kv: 8 (over z, y), tp: 4 (over x, core).
Axes of the slice: x: 2, y: 2, z: 4, core: 2. Of those that a mesh axis runs over, the one named last changes fastest.
Arguments:
- queries: bfloat16 [1024, 1024], P('kv', 'tp'), may hold values from -6 to 6
- keys: bfloat16 [1024, 512], P('kv', 'tp'), may hold values from -6 to 6
- values: bfloat16 [1024, 512], P('kv', 'tp'), may hold values from -6 to 6
- hidden: bfloat16 [1024, 2048], P('kv'), may hold values from -6 to 6
- log_sums: float32 [2, 1024, 16], P(None, 'kv', 'tp'), may hold values from -1 to 12
- gates: float32 [2, 1024, 16], P(None, 'kv', 'tp'), may hold values from 0.1 to 0.9
- branch_out: bfloat16 [2, 1024, 1024], P(None, 'kv', 'tp'), may hold values from -6 to 6
- cotangent: bfloat16 [1024, 1024], P('kv', 'tp'), may hold values from -6 to 6
- chosen: int32 [8, 8, 48], P(None, 'tp'), may hold values from -1 to 31, as said below
Outputs:
- grad_queries: float32 [1024, 1024], P('kv', 'tp')
- grad_keys: float32 [1024, 512], P('kv', 'tp')
- grad_values: float32 [1024, 512], P('kv', 'tp')
- grad_weight: float32 [2048, 1024], P('kv', 'tp')
Inputs may be any that keep to these rules, and one draw needn't show every extreme that they name: `chosen`: each list holds global block numbers or -1. All live entries of one list name blocks of distinct owners, owner = entry // 4, none later than the list's range; list d holds min(48, d + 1) live entries, and they come first.
All inputs are finite; a program needn't handle non-finite values.
Results may differ from a plain program's by a relative error of at most 0.0055.
Values may be sent and summed in bfloat16 or wider, within the bound.
A program may use at most 64 MiB of HBM per device.

v0:
```python
import jax
import jax.numpy as jnp
from jax import lax
from jax.sharding import PartitionSpec as P

DH = 64
BLK = 32
TOPN = 12
SUB = 4
CMP = 32


def branch_grads(query_rows, key_rows, value_rows, seen, log_rows, delta_rows, cot_rows, scale):
    wide = jnp.float32
    scores = jnp.einsum("tgre,gme->grtm", query_rows, key_rows, preferred_element_type=wide) * scale
    log_here = jnp.transpose(log_rows, (1, 2, 0))[..., None]
    delta_here = jnp.transpose(delta_rows, (1, 2, 0))[..., None]
    probs = jnp.where(seen[:, None], jnp.exp(scores - log_here), 0.0)
    probs_low = probs.astype(jnp.bfloat16)
    value_grad = jnp.einsum("grtm,tgre->gme", probs_low, cot_rows, preferred_element_type=wide)
    prob_grad = jnp.einsum("tgre,gme->grtm", cot_rows, value_rows, preferred_element_type=wide)
    score_low = (probs * (prob_grad - delta_here)).astype(jnp.bfloat16)
    query_grad = (
        jnp.einsum("grtm,gme->tgre", score_low, key_rows, preferred_element_type=wide) * scale
    )
    key_grad = (
        jnp.einsum("grtm,tgre->gme", score_low, query_rows, preferred_element_type=wide) * scale
    )
    return (query_grad, key_grad, value_grad)


def shards(queries, keys, values, hidden, log_sums, gates, branch_out, cotangent, chosen):
    wide = jnp.float32
    rows_here = queries.shape[0]
    heads = queries.shape[1] // DH
    groups = keys.shape[1] // DH
    group_heads = heads // groups
    per_block = rows_here // BLK
    per_summary = rows_here // CMP
    blocks_all = chosen.shape[0]
    nsel = chosen.shape[2]
    qrows = rows_here // SUB
    scale = DH ** (-0.5)
    grads_each = jax.vmap(branch_grads, in_axes=(0, 0, 0, 0, 0, 0, 0, None))
    place = lax.axis_index("kv")
    position = place * rows_here + jnp.arange(rows_here, dtype=jnp.int32)
    gated = gates[..., None] * cotangent.reshape(rows_here, heads, DH).astype(wide)[None]
    delta_all = jnp.sum(gated * branch_out.reshape(2, rows_here, heads, DH).astype(wide), -1)
    delta_all = delta_all.reshape(2, rows_here, groups, group_heads)
    gated_low = gated.astype(jnp.bfloat16).reshape(2, rows_here, groups, group_heads, DH)
    log_all = log_sums.reshape(2, rows_here, groups, group_heads)
    query_all = queries.reshape(rows_here, groups, group_heads, DH)
    pairs = jnp.concatenate(
        [keys.reshape(rows_here, groups, DH), values.reshape(rows_here, groups, DH)], -1
    )
    means = jnp.mean(pairs.reshape(per_summary, CMP, groups, 2 * DH).astype(wide), 1).astype(
        jnp.bfloat16
    )
    summaries = lax.all_gather(means, "kv", axis=0, tiled=True)
    summary_count = summaries.shape[0]
    sum_keys = jnp.transpose(summaries[..., :DH], (1, 0, 2))
    sum_values = jnp.transpose(summaries[..., DH:], (1, 0, 2))
    summary_end = jnp.arange(summary_count, dtype=jnp.int32) * CMP + CMP - 1
    summary_seen = (summary_end[None, :] <= position[:, None])[None]
    query_sum, key_sum, value_sum = branch_grads(
        query_all, sum_keys, sum_values, summary_seen, log_all[0], delta_all[0], gated_low[0], scale
    )
    summary_term = jnp.transpose(jnp.concatenate([key_sum, value_sum], -1), (1, 0, 2))
    listing = lax.dynamic_index_in_dim(chosen, place, 0, keepdims=False)
    live = listing >= 0
    safe = jnp.maximum(listing, 0)
    owner = safe // per_block
    group_index = jnp.arange(groups, dtype=jnp.int32)
    hits = (chosen >= 0) & (chosen // per_block == place)
    wanted = jnp.sum(jnp.where(hits, chosen % per_block, 0), -1)
    asked = jnp.any(hits, -1)
    row_target = safe[..., None] * BLK + jnp.arange(BLK, dtype=jnp.int32)
    pair_blocks = pairs.reshape(per_block, BLK, groups, 2 * DH)
    outbound = pair_blocks[wanted, :, group_index[None, :], :]
    arrived = lax.all_to_all(outbound, "kv", split_axis=0, concat_axis=0, tiled=True)
    picked = arrived[owner, group_index[:, None]]

    def by_sub(array):
        rest = array.shape[3:]
        moved = array.reshape((groups, SUB, TOPN * BLK) + rest)
        return jnp.swapaxes(moved, 0, 1)

    picked_sub = by_sub(picked)
    picked_keys = picked_sub[..., :DH]
    picked_values = picked_sub[..., DH:]
    live_rows = by_sub(jnp.broadcast_to(live[..., None], (groups, nsel, BLK)))
    key_position = by_sub(row_target)
    sub_position = position.reshape(SUB, qrows)
    block_seen = live_rows[:, :, None, :] & (
        key_position[:, :, None, :] <= sub_position[:, None, :, None]
    )
    query_sel, key_sel, value_sel = grads_each(
        query_all.reshape(SUB, qrows, groups, group_heads, DH),
        picked_keys,
        picked_values,
        block_seen,
        log_all[1].reshape(SUB, qrows, groups, group_heads),
        delta_all[1].reshape(SUB, qrows, groups, group_heads),
        gated_low[1].reshape(SUB, qrows, groups, group_heads, DH),
        scale,
    )
    query_sel = query_sel.reshape(rows_here, groups, group_heads, DH)
    key_sel = jnp.swapaxes(key_sel, 0, 1).reshape(groups, nsel, BLK, DH)
    value_sel = jnp.swapaxes(value_sel, 0, 1).reshape(groups, nsel, BLK, DH)
    slot_grads = jnp.concatenate([key_sel, value_sel], -1)
    slot_grads = slot_grads * live[..., None, None].astype(wide)
    outgoing = (
        jnp.zeros((blocks_all, groups, BLK, 2 * DH), wide)
        .at[owner, group_index[:, None]]
        .add(slot_grads)
    )
    summary_out = jnp.transpose(
        summary_term.reshape(blocks_all, per_summary, groups, 2 * DH), (0, 2, 1, 3)
    )
    both_out = jnp.concatenate([outgoing, summary_out], 2)
    both_in = lax.all_to_all(
        both_out.astype(jnp.bfloat16), "kv", split_axis=0, concat_axis=0, tiled=True
    ).astype(both_out.dtype)
    incoming = both_in[:, :, :BLK]
    summary_mine = jnp.transpose(jnp.sum(both_in[:, :, BLK:], 0), (1, 0, 2))
    selector = (
        (wanted[..., None] == jnp.arange(per_block, dtype=jnp.int32)) & asked[..., None]
    ).astype(wide)
    block_sums = jnp.einsum("rgb,rgkc->bkgc", selector, incoming, precision=lax.Precision.HIGHEST)
    pair_grads = (
        block_sums.reshape(rows_here, groups, 2 * DH) + jnp.repeat(summary_mine, CMP, axis=0) / CMP
    )
    grad_queries = (query_sum + query_sel).reshape(rows_here, heads * DH)
    query_low = grad_queries.astype(jnp.bfloat16)
    grad_weight = lax.psum_scatter(
        lax.dot_general(
            hidden, query_low, (((0,), (0,)), ((), ())), preferred_element_type=jnp.float32
        ),
        "kv",
        scatter_dimension=0,
        tiled=True,
    )
    grad_keys = pair_grads[..., :DH].reshape(rows_here, groups * DH)
    grad_values = pair_grads[..., DH:].reshape(rows_here, groups * DH)
    return (grad_queries, grad_keys, grad_values, grad_weight)


def solution(mesh):
    return jax.shard_map(
        shards,
        mesh=mesh,
        in_specs=(
            P("kv", "tp"),
            P("kv", "tp"),
            P("kv", "tp"),
            P("kv", None),
            P(None, "kv", "tp"),
            P(None, "kv", "tp"),
            P(None, "kv", "tp"),
            P("kv", "tp"),
            P(None, "tp", None),
        ),
        out_specs=(P("kv", "tp"), P("kv", "tp"), P("kv", "tp"), P("kv", "tp")),
        check_vma=False,
    )
```

profile of v0, /device:TPU:0, one launch (start us, length us, event | category | flops | bytes accessed | tf_op | source)
XLA Modules:
  0.0 135.9 jit_solution(15902463175480948571)
XLA Ops:
  7.2 1.0 fusion.44
  8.2 0.9 fusion.33
  9.1 0.1 copy.157
  9.2 0.1 copy.158
  9.3 0.1 reshape.249
  9.4 0.8 concatenate.26
  10.3 0.8 concatenate.27
  11.1 0.1 convert_reduce_fusion
  11.3 1.3 gather_fusion
  12.5 7.3 %all-to-all-start = ((bf16[8,2,32,128]{3,2,1,0:T(8,128)(2,1)}), bf16[8,2,32,128]{3,2,1,0:T(8,128)(2,1)S(1)}, u32[]{:S(2)}, u32[]{:S(2)}) async-start(bf16[8,2,32,128]{3,2,1,0:T(8,128)(2,1)} %bitcast.20), calls=%async_computation | async-start | bytes 262144 | tf_op jit(solution)/shard_map/all_to_all | solution.py:80
  19.9 0.7 multiply_bitcast_fusion.1
  20.6 0.7 fusion.45
  21.3 0.7 or_select_fusion
  22.0 1.0 copy.153
  22.9 1.0 reshape_reshape.3
  23.9 0.1 reshape.255
  24.0 0.1 add.117
  24.1 0.1 broadcast_in_dim.36
  24.2 0.1 reshape.239
  24.4 0.1 add.115
  24.5 26.6 %all_gather.3 = bf16[32,2,128]{2,1,0:T(2,128)(2,1)S(1)} all-gather(bf16[4,2,128]{2,1,0:T(2,128)(2,1)S(1)} %multiply_convert_fusion.1), channel_id=1, replica_groups=mesh['kv'=8,'tp'=4] {'kv'}, dimensions={0}, use_global_device_ids=true | all-gather | bytes 18432 | tf_op jit(solution)/shard_map/all_gather | solution.py:59
  51.1 0.1 fusion.48
  51.2 0.1 copy.155
  51.4 0.1 copy.156
  51.7 0.1 compare_and_fusion
  51.8 0.1 fusion.18
  52.0 0.1 reshape_squeeze.9
  52.1 0.1 reshape_squeeze.11
  52.2 0.1 copy.164
  52.3 0.1 fusion.19
  52.4 1.2 gather_fusion.1
  53.6 0.4 copy.159
  54.0 0.3 fusion.5
  54.3 0.3 fusion.8
  54.6 0.3 fusion.9
  54.9 0.3 copy-done.1
  55.2 0.1 copy.168
  55.3 0.2 fusion.12
  55.5 1.8 %convolution_bitcast_fusion = f32[2048,256]{0,1:T(8,128)} fusion(bf16[128,2048]{1,0:T(8,128)(2,1)S(1)} %copy-done, f32[128,256]{0,1:T(8,128)S(1)} %bitcast.188), kind=kOutput, calls=%fused_computation.3 | convolution fusion | flops 134250496 | bytes 2752512 | tf_op jit(solution)/shard_map/dot_general | solution.py:136
  57.3 0.1 reshape.261
  57.4 0.1 fusion.21
  57.5 0.1 fusion.22
  57.7 0.1 pad_maximum_fusion.2
  57.8 0.4 copy-done.3
  58.2 0.3 fusion.7
  58.5 0.5 copy.170
  59.0 1.4 %convolution_bitcast_fusion.1 = f32[2,4,384,64]{2,3,0,1:T(8,128)S(1)} fusion(f32[4,2,2,32,384]{4,3,2,1,0:T(8,128)} %copy-done.1, bf16[4,32,2,2,64]{4,1,0,3,2:T(8,128)(2,1)S(1)} %bitcast.187), kind=kOutput, calls=%fused_computation.5 | convolution fusion | flops 25362432 | bytes 1638400 | tf_op jit(solution)/shard_map/vmap(grtm,tgre->gme)/dot_general | solution.py:20
  60.4 1.6 %copy.172 = f32[2,4,384,64]{3,2,1,0:T(8,128)} copy(f32[2,4,384,64]{2,3,0,1:T(8,128)S(1)} %convolution_bitcast_fusion.1) | data formatting | bytes 1572864 | tf_op jit(solution)/shard_map/transpose | solution.py:109
  62.1 3.2 %maximum_multiply_fusion = f32[2,48,32,128]{3,2,1,0:T(8,128)} fusion(f32[2,48,32,64]{3,2,1,0:T(8,128)} %bitcast.180, f32[2,48,32,64]{3,2,1,0:T(8,128)S(1)} %bitcast.178, f32[2,48]{1,0:T(2,128)S(1)} %get-tuple-element.30), kind=kLoop, calls=%fused_computation.4 | loop fusion | flops 786432 | bytes 3146112 | tf_op jit(solution)/shard_map/mul | solution.py:111
  65.3 9.7 %scatter_fusion = f32[8,2,32,128]{3,2,1,0:T(8,128)S(1)} fusion(f32[8,2,32,128]{3,2,1,0:T(8,128)S(1)} %broadcast_in_dim.39, s32[96]{0:T(128)S(1)} %reshape.261, f32[96,32,128]{2,1,0:T(8,128)} %bitcast.179), kind=kCustom, calls=%fused_computation.2 | custom fusion | flops 393216 | bytes 4719360 | tf_op jit(solution)/shard_map/scatter-add | solution.py:115
  75.1 0.8 copy.174
  75.9 3.9 %all-to-all-start.1 = ((bf16[8,2,36,128]{3,1,2,0:T(2,128)(2,1)}), bf16[8,2,36,128]{3,1,2,0:T(2,128)(2,1)S(1)}, u32[]{:S(2)}, u32[]{:S(2)}) async-start(bf16[8,2,36,128]{3,1,2,0:T(2,128)(2,1)} %copy.174), calls=%async_computation.1 | async-start | bytes 294912 | tf_op jit(solution)/shard_map/all_to_all | solution.py:121
  79.8 0.1 copy.177
  79.9 0.8 copy.182
  80.6 8.6 %all-to-all-done.1 = bf16[8,2,36,128]{3,1,2,0:T(2,128)(2,1)S(1)} async-done(((bf16[8,2,36,128]{3,1,2,0:T(2,128)(2,1)}), bf16[8,2,36,128]{3,1,2,0:T(2,128)(2,1)S(1)}, u32[]{:S(2)}, u32[]{:S(2)}) %all-to-all-start.1) | async-done | bytes 147488 | tf_op jit(solution)/shard_map/all_to_all | solution.py:121
  89.2 0.1 slice.80
  89.3 0.3 fusion.10
  89.6 0.1 fusion.46
  89.7 0.1 copy.181
  89.8 0.7 copy.184
  90.5 0.1 copy.180
  90.6 0.7 copy.183
  91.4 35.9 %reduce-scatter.2.cloned.1.call-done = f32[256,256]{0,1:T(8,128)} async-done(((f32[2048,256]{0,1:T(8,128)}), f32[256,256]{0,1:T(8,128)}) %reduce-scatter.2.cloned.1.call-update) | async-done | bytes 262160 | tf_op jit(solution)/shard_map/reduce_scatter | solution.py:135
  127.3 1.8 %copy.185 = f32[256,256]{1,0:T(8,128)} copy(f32[256,256]{0,1:T(8,128)} %reduce-scatter.2.cloned.1.call-done) | data formatting | bytes 524288
  (47 shorter events, 0.6 us)
Async XLA Ops:
  7.2 48.4 %copy-start = (bf16[128,2048]{1,0:T(8,128)(2,1)S(1)}, bf16[128,2048]{1,0:T(8,128)(2,1)}, u32[]{:S(2)}) copy-start(bf16[128,2048]{1,0:T(8,128)(2,1)} %param.12) | copy-start | bytes 1572868
  7.2 16.8 %copy-start.7 = (f32[2,128,4]{1,2,0:T(4,128)S(1)}, f32[2,128,4]{1,2,0:T(4,128)}, u32[]{:S(2)}) copy-start(f32[2,128,4]{1,2,0:T(4,128)} %param.13) | copy-start | bytes 12292
  7.2 44.0 %copy-start.5 = (bf16[128,256]{1,0:T(8,128)(2,1)S(1)}, bf16[128,256]{1,0:T(8,128)(2,1)}, u32[]{:S(2)}) copy-start(bf16[128,256]{1,0:T(8,128)(2,1)} %param.16) | copy-start | bytes 196612
  7.2 44.2 %copy-start.4 = (bf16[2,128,256]{2,1,0:T(8,128)(2,1)S(1)}, bf16[2,128,256]{2,1,0:T(8,128)(2,1)}, u32[]{:S(2)}) copy-start(bf16[2,128,256]{2,1,0:T(8,128)(2,1)} %param.15) | copy-start | bytes 393220
  7.2 44.3 %copy-start.6 = (f32[2,128,4]{1,2,0:T(4,128)S(1)}, f32[2,128,4]{1,2,0:T(4,128)}, u32[]{:S(2)}) copy-start(f32[2,128,4]{1,2,0:T(4,128)} %param.14) | copy-start | bytes 12292
  12.5 39.9 %all-to-all-start = ((bf16[8,2,32,128]{3,2,1,0:T(8,128)(2,1)}), bf16[8,2,32,128]{3,2,1,0:T(8,128)(2,1)S(1)}, u32[]{:S(2)}, u32[]{:S(2)}) async-start(bf16[8,2,32,128]{3,2,1,0:T(8,128)(2,1)} %bitcast.20), calls=%async_computation | async-start | bytes 262144 | tf_op jit(solution)/shard_map/all_to_all | solution.py:80
  19.8 107.5 %reduce-scatter.2.cloned.1.call-start = ((), (), s32[]{:S(2)}) async-start(), calls=%async_computation.3 | async-start | bytes 2359296 | tf_op jit(solution)/shard_map/reduce_scatter | solution.py:135
  23.9 30.1 %copy-start.2 = (bf16[4,32,2,2,64]{4,3,2,1,0:T(2,128)(2,1)}, bf16[4,32,2,2,64]{4,3,2,1,0:T(2,128)(2,1)S(1)}, u32[]{:S(2)}) copy-start(bf16[4,32,2,2,64]{4,3,2,1,0:T(2,128)(2,1)S(1)} %reshape_reshape.3) | copy-start | bytes 196612
  54.3 0.9 copy-start.1
  57.3 0.9 copy-start.3
  75.9 13.3 %all-to-all-start.1 = ((bf16[8,2,36,128]{3,1,2,0:T(2,128)(2,1)}), bf16[8,2,36,128]{3,1,2,0:T(2,128)(2,1)S(1)}, u32[]{:S(2)}, u32[]{:S(2)}) async-start(bf16[8,2,36,128]{3,1,2,0:T(2,128)(2,1)} %copy.174), calls=%async_computation.1 | async-start | bytes 294912 | tf_op jit(solution)/shard_map/all_to_all | solution.py:121
Sparse Core Ops, SparseCore 0:
  57.4 69.8 reduce-scatter.1
where the time goes:
time: 137 us; the launch traced here: 136 us
  waiting for transfers between devices  44.5 us (32%)
  blocking collectives  26.6 us (19%)
  other arithmetic  17.5 us (13%)
  local copies, waits for them, and re-layouts  16.2 us (12%)
  between operations  14.5 us (11%)
  starting transfers between devices  11.3 us (8%)
  matrix products  5.35 us (4%)
    reduce_scatter x1, waiting for transfers between devices, shards(): lax.psum_scatter(lax.dot_general(hidden, query_low, (((0,), (0,)), ((), (...  35.9 us
    all_gather x1, blocking collectives, shards(): summaries = lax.all_gather(means, 'kv', axis=0, tiled=True)  26.6 us
    scatter-add x1, other arithmetic, shards(): outgoing = jnp.zeros((blocks_all, groups, BLK, 2 * DH), wide).at[owner, g...  9.74 us
    all_to_all x1, waiting for transfers between devices, shards(): lax.all_to_all(both_out.astype(jnp.bfloat16), 'kv', split_axis=0, concat_...  8.57 us
    all_to_all x1, starting transfers between devices, shards(): lax.all_to_all(outbound, 'kv', split_axis=0, concat_axis=0, tiled=True)  7.31 us
    unnamed x23, local copies, waits for them, and re-layouts  5.95 us
    all_to_all x1, starting transfers between devices, shards(): lax.all_to_all(both_out.astype(jnp.bfloat16), 'kv', split_axis=0, concat_...  3.92 us
    mul x1, other arithmetic, shards(): slot_grads = slot_grads * live[..., None, None].astype(wide)  3.19 us
  transfers between devices with their start and end apart: 3, of which 2 were waited for; matrix products, arithmetic and copies ran while one was open for 20% of the time, Pallas kernels for 0%

commit v1 on v0

--- a/solution.py
+++ b/solution.py
@@ -1,6 +1,10 @@
+import functools
+
 import jax
 import jax.numpy as jnp
 from jax import lax
+from jax.experimental import pallas as pl
+from jax.experimental.pallas import tpu as pltpu
 from jax.sharding import PartitionSpec as P
 
 DH = 64
@@ -145,9 +149,265 @@
     return (grad_queries, grad_keys, grad_values, grad_weight)
 
 
+WIDE = jnp.float32
+LOW = jnp.bfloat16
+NT = (((1,), (1,)), ((), ()))
+TN = (((0,), (0,)), ((), ()))
+NN = (((1,), (0,)), ((), ()))
+
+
+def dot(a, b, dims):
+    return lax.dot_general(a, b, dims, preferred_element_type=WIDE)
+
+
+def fused_kernel(
+    n, q_ref, k_ref, v_ref, hid_ref, log_ref, gate_ref, out_ref, cot_ref, chosen_ref,
+    gq_ref, gk_ref, gv_ref, gw_ref,
+    table, blk_out, blk_in, grd_out, grd_in, qb_out, qb_in, hid_in, hid_t,
+    blk_send, blk_recv, hid_send, hid_recv, qb_send, qb_recv, grd_send, grd_recv, own_sem,
+):
+    rows, width = q_ref.shape
+    heads = width // DH
+    lanes = k_ref.shape[1]
+    groups = lanes // DH
+    group_heads = heads // groups
+    per_block = rows // BLK
+    per_summary = rows // CMP
+    pad = blk_in.shape[1] // 2 - BLK
+    qrows = rows // SUB
+    cols = hid_in.shape[2]
+    scale = DH ** (-0.5)
+    me = lax.axis_index("kv")
+    to = [lax.rem(me + s, n) for s in range(n)]
+
+    def copy(src, dst, send, recv, peer):
+        return pltpu.make_async_remote_copy(
+            src_ref=src, dst_ref=dst, send_sem=send, recv_sem=recv,
+            device_id={"kv": peer}, device_id_type=pl.DeviceIdType.MESH,
+        )
+
+    barrier = pltpu.get_barrier_semaphore()
+    for s in range(1, n):
+        pl.semaphore_signal(
+            barrier, inc=1, device_id={"kv": to[s]}, device_id_type=pl.DeviceIdType.MESH
+        )
+
+    def hidden_of(peer):
+        return hid_ref.at[:, pl.ds(pl.multiple_of(peer * cols, cols), cols)]
+
+    own_hidden = pltpu.make_async_copy(hidden_of(me), hid_in.at[0], own_sem)
+    own_hidden.start()
+
+    lane_group = lax.broadcasted_iota(jnp.int32, (n, lanes), 1) // DH
+    wanted = jnp.zeros((n, lanes), WIDE)
+    for g in range(groups):
+        listing = chosen_ref[:, g, :]
+        hit = (listing >= me * per_block) & (listing < (me + 1) * per_block)
+        inner = jnp.where(hit, (listing - me * per_block).astype(WIDE), 0.0)
+        wanted = jnp.where(lane_group == g, jnp.sum(inner, -1, keepdims=True), wanted)
+    table[...] = wanted
+    want = [table[pl.ds(to[s], 1), :] for s in range(n)]
+
+    keys = k_ref[...].astype(WIDE)
+    values = v_ref[...].astype(WIDE)
+
+    def summary_of(array):
+        row = lax.broadcasted_iota(jnp.int32, (pad, lanes), 0)
+        result = jnp.zeros((pad, lanes), WIDE)
+        for j in range(per_summary):
+            mean = jnp.sum(array[j * CMP : (j + 1) * CMP], 0, keepdims=True) / CMP
+            result = jnp.where(row == j, mean, result)
+        return result.astype(LOW)
+
+    def block_of(array, row):
+        result = array[:BLK]
+        for b in range(1, per_block):
+            result = jnp.where(row == b, array[b * BLK : (b + 1) * BLK], result)
+        return result.astype(LOW)
+
+    sum_keys = summary_of(keys)
+    sum_values = summary_of(values)
+    for s in range(n):
+        target = blk_in if s == 0 else blk_out
+        target[s, :BLK] = block_of(keys, want[s])
+        target[s, BLK : 2 * BLK] = block_of(values, want[s])
+        target[s, 2 * BLK : 2 * BLK + pad] = sum_keys
+        target[s, 2 * BLK + pad :] = sum_values
+
+    pl.semaphore_wait(barrier, n - 1)
+    blk = [
+        copy(blk_out.at[s], blk_in.at[s], blk_send.at[s], blk_recv.at[s], to[s]) for s in range(1, n)
+    ]
+    for c in blk:
+        c.start()
+    hid = [
+        copy(hidden_of(to[s]), hid_in.at[s], hid_send.at[s], hid_recv.at[s], to[s])
+        for s in range(1, n)
+    ]
+    for c in hid:
+        c.start()
+
+    def head_stats(branch, h, count):
+        at = slice(h * DH, (h + 1) * DH)
+        gated = gate_ref[branch, :count, h : h + 1] * cot_ref[:count, at].astype(WIDE)
+        delta = jnp.sum(gated * out_ref[branch, :count, at].astype(WIDE), -1, keepdims=True)
+        return gated.astype(LOW), delta, log_ref[branch, :count, h : h + 1], q_ref[:count, at]
+
+    def stats(branch, g, count):
+        each = [head_stats(branch, g * group_heads + r, count) for r in range(group_heads)]
+        return [jnp.concatenate(part, 0) for part in zip(*each)]
+
+    prepared = [(stats(0, g, rows), stats(1, g, qrows)) for g in range(groups)]
+
+    def owner_of(shape, per_slot):
+        slot = lax.broadcasted_iota(jnp.int32, shape, 1)
+        return lax.rem(me - slot // per_slot + n, n), slot % per_slot
+
+    shape0 = (group_heads * rows, n * pad)
+    owner0, inner0 = owner_of(shape0, pad)
+    time0 = me * rows + lax.broadcasted_iota(jnp.int32, shape0, 0) % rows
+    seen0 = (inner0 < per_summary) & ((owner0 * per_summary + inner0 + 1) * CMP - 1 <= time0)
+    shape1 = (group_heads * qrows, n * BLK)
+    owner1, inner1 = owner_of(shape1, BLK)
+    time1 = lax.broadcasted_iota(jnp.int32, shape1, 0) % qrows
+
+    def branch(query, key, value, seen, low, delta, log):
+        probs = jnp.where(seen, jnp.exp(dot(query, key, NT) * scale - log), 0.0)
+        score = (probs * (dot(low, value, NT) - delta)).astype(LOW)
+        return probs.astype(LOW), score
+
+    for c in blk:
+        c.wait_recv()
+    all_keys = blk_in[:, :BLK].reshape(n * BLK, lanes)
+    all_values = blk_in[:, BLK : 2 * BLK].reshape(n * BLK, lanes)
+    all_sum_keys = blk_in[:, 2 * BLK : 2 * BLK + pad].reshape(n * pad, lanes)
+    all_sum_values = blk_in[:, 2 * BLK + pad :].reshape(n * pad, lanes)
+    probs_all, score_all, grads = [], [], []
+    for g in range(groups):
+        at = slice(g * DH, (g + 1) * DH)
+        (low0, delta0, log0, query0), (low1, delta1, log1, query1) = prepared[g]
+        own_block = want[0][:, g * DH : g * DH + 1]
+        first = own_block * BLK + inner1.astype(WIDE) <= time1.astype(WIDE)
+        seen1 = (owner1 < me) | ((owner1 == me) & first)
+        probs0, score0 = branch(query0, all_sum_keys[:, at], all_sum_values[:, at], seen0, low0, delta0, log0)
+        probs1, score1 = branch(query1, all_keys[:, at], all_values[:, at], seen1, low1, delta1, log1)
+        grad0 = dot(score0, all_sum_keys[:, at], NN) * scale
+        grad1 = dot(score1, all_keys[:, at], NN) * scale
+        for r in range(group_heads):
+            h = slice((g * group_heads + r) * DH, (g * group_heads + r + 1) * DH)
+            start = r * rows
+            top = grad0[start : start + qrows] + grad1[r * qrows : (r + 1) * qrows]
+            gq_ref[:qrows, h] = top
+            gq_ref[qrows:, h] = grad0[start + qrows : start + rows]
+        probs_all.append((probs0, probs1))
+        score_all.append((score0, score1))
+    qb_out[...] = gq_ref[...].astype(LOW)
+    qb = [copy(qb_out, qb_in.at[s], qb_send.at[s], qb_recv.at[s], to[s]) for s in range(1, n)]
+
+    def wide_of(parts):
+        return jnp.concatenate(parts, 1)
+
+    key1 = wide_of([dot(score_all[g][1], prepared[g][1][3], TN) for g in range(groups)]) * scale
+    value1 = wide_of([dot(probs_all[g][1], prepared[g][1][0], TN) for g in range(groups)])
+    key0 = wide_of([dot(score_all[g][0], prepared[g][0][3], TN) for g in range(groups)]) * scale
+    value0 = wide_of([dot(probs_all[g][0], prepared[g][0][0], TN) for g in range(groups)])
+    for s in range(1, n):
+        grd_out[s, :BLK] = key1[s * BLK : (s + 1) * BLK].astype(LOW)
+        grd_out[s, BLK : 2 * BLK] = value1[s * BLK : (s + 1) * BLK].astype(LOW)
+        grd_out[s, 2 * BLK : 2 * BLK + pad] = key0[s * pad : (s + 1) * pad].astype(LOW)
+        grd_out[s, 2 * BLK + pad :] = value0[s * pad : (s + 1) * pad].astype(LOW)
+    grd = [
+        copy(grd_out.at[s], grd_in.at[s], grd_send.at[s], grd_recv.at[s], to[n - s])
+        for s in range(1, n)
+    ]
+    for c in qb:
+        c.start()
+    for c in grd:
+        c.start()
+
+    own_hidden.wait()
+    hid_t[0] = hid_in[0].T
+    total = dot(hid_t[0], qb_out[...], NN)
+    for s in range(1, n):
+        hid[s - 1].wait_recv()
+        hid_t[s] = hid_in[s].T
+
+    for c in grd:
+        c.wait_recv()
+    for block_part, sum_part, own_block, own_sum, result in (
+        (0, 2 * BLK, key1, key0, gk_ref),
+        (BLK, 2 * BLK + pad, value1, value0, gv_ref),
+    ):
+        here = [own_block[:BLK]]
+        summed = own_sum[:pad]
+        for s in range(1, n):
+            here.append(grd_in[s, block_part : block_part + BLK].astype(WIDE))
+            summed = summed + grd_in[s, sum_part : sum_part + pad].astype(WIDE)
+        for b in range(per_block):
+            block = jnp.zeros((BLK, lanes), WIDE)
+            for s in range(n):
+                block = block + jnp.where(want[s] == b, here[s], 0.0)
+            for j in range(BLK // CMP):
+                at = b * BLK + j * CMP
+                term = summed[at // CMP : at // CMP + 1] / CMP
+                result[at : at + CMP] = block[j * CMP : (j + 1) * CMP] + term
+
+    for s in range(1, n):
+        qb[s - 1].wait_recv()
+        total = total + dot(hid_t[s], qb_in[s], NN)
+    gw_ref[...] = total
+    for c in blk + hid + qb + grd:
+        c.wait_send()
+
+
+def fused(n, queries, keys, values, hidden, log_sums, gates, branch_out, cotangent, chosen):
+    rows, width = queries.shape
+    lanes = keys.shape[1]
+    cols = hidden.shape[1] // n
+    pad = -(-(rows // CMP) // 16) * 16
+    size = 2 * (BLK + pad)
+    vmem = pl.BlockSpec(memory_space=pltpu.VMEM)
+    sems = pltpu.SemaphoreType.DMA((n,))
+    return pl.pallas_call(
+        functools.partial(fused_kernel, n),
+        out_shape=(
+            jax.ShapeDtypeStruct((rows, width), WIDE),
+            jax.ShapeDtypeStruct((rows, lanes), WIDE),
+            jax.ShapeDtypeStruct((rows, lanes), WIDE),
+            jax.ShapeDtypeStruct((cols, width), WIDE),
+        ),
+        in_specs=[vmem] * 3 + [pl.BlockSpec(memory_space=pl.ANY)] + [vmem] * 5,
+        out_specs=(vmem,) * 4,
+        scratch_shapes=[
+            pltpu.VMEM((n, lanes), WIDE),
+            pltpu.VMEM((n, size, lanes), LOW),
+            pltpu.VMEM((n, size, lanes), LOW),
+            pltpu.VMEM((n, size, lanes), LOW),
+            pltpu.VMEM((n, size, lanes), LOW),
+            pltpu.VMEM((rows, width), LOW),
+            pltpu.VMEM((n, rows, width), LOW),
+            pltpu.VMEM((n, rows, cols), LOW),
+            pltpu.VMEM((n, cols, rows), LOW),
+            sems, sems, sems, sems, sems, sems, sems, sems,
+            pltpu.SemaphoreType.DMA,
+        ],
+        compiler_params=pltpu.CompilerParams(collective_id=0, has_side_effects=True),
+    )(queries, keys, values, hidden, log_sums, gates, branch_out, cotangent, chosen)
+
+
+def fits(n, hidden, chosen):
+    return chosen.shape[0] <= TOPN and (hidden.shape[1] // n) % 128 == 0
+
+
 def solution(mesh):
+
+    n = mesh.shape["kv"]
+
+    def body(*args):
+        return fused(n, *args) if fits(n, args[3], args[8]) else shards(*args)
+
     return jax.shard_map(
-        shards,
+        body,
         mesh=mesh,
         in_specs=(
             P("kv", "tp"),

time: 137 us -> 48.6 us (0.35)
  waiting for transfers between devices: 44.5 us -> 0 us
  Pallas kernels: 0 us -> 41.6 us
  blocking collectives: 26.6 us -> 0 us
  other arithmetic: 17.5 us -> 0 us
  between operations: 14.5 us -> 0.67 us
  starting transfers between devices: 11.3 us -> 0 us
  local copies, waits for them, and re-layouts: 16.2 us -> 6.11 us
  matrix products: 5.35 us -> 0 us
    pallas_call x0 -> x1, Pallas kernels: none -> 41.6 us  [fused(): pl.pallas_call(functools.partial(fused_kernel, n), out_shape=(jax.ShapeDt...]
    reduce_scatter x1 -> x0, waiting for transfers between devices: 35.9 us -> none  [shards(): lax.psum_scatter(lax.dot_general(hidden, query_low, (((0,), (0,)), ((), (...]
    all_gather x1 -> x0, blocking collectives: 26.6 us -> none  [shards(): summaries = lax.all_gather(means, 'kv', axis=0, tiled=True)]
    all_to_all x2 -> x0, starting transfers between devices: 11.2 us -> none  [the longest x1 7.31 us: shards(): lax.all_to_all(outbound, 'kv', split_axis=0, concat_axis=0, tiled=True)]
    scatter-add x1 -> x0, other arithmetic: 9.74 us -> none  [shards(): outgoing = jnp.zeros((blocks_all, groups, BLK, 2 * DH), wide).at[owner, g...]
    all_to_all x2 -> x0, waiting for transfers between devices: 8.57 us -> none  [the longest x1 8.57 us: shards(): lax.all_to_all(both_out.astype(jnp.bfloat16), 'kv', split_axis=0, concat_...]
    dot_general x12 -> x0, matrix products: 5.35 us -> none  [the longest x1 1.75 us: shards(): lax.dot_general(hidden, query_low, (((0,), (0,)), ((), ())), preferred_el...]
    mul x2 -> x0, other arithmetic: 3.88 us -> none  [the longest x1 3.19 us: shards(): slot_grads = slot_grads * live[..., None, None].astype(wide)]
  transfers between devices with their start and end apart: 3 -> 0, of which waited for: 2 -> 0; matrix products, arithmetic and copies ran while one was open for 20% -> 0% of each run, Pallas kernels for 0% -> 0%
where the time goes in v1:
time: 48.6 us; the launch traced here: 48.3 us
  Pallas kernels  41.6 us (86%)
  local copies, waits for them, and re-layouts  6.11 us (13%)
  between operations  0.67 us (1%)
    pallas_call x1, Pallas kernels, fused(): pl.pallas_call(functools.partial(fused_kernel, n), out_shape=(jax.ShapeDt...  41.6 us
    unnamed x14, local copies, waits for them, and re-layouts  6.11 us

profile of v1, /device:TPU:0, one launch (start us, length us, event | category | flops | bytes accessed | tf_op | source)
XLA Modules:
  0.0 48.3 jit_solution(4108968119152664129)
XLA Ops:
  0.6 0.0 copy-start.3
  0.6 1.5 %copy.13.log_ref = f32[2,128,4]{2,1,0:T(8,128)} copy(f32[2,128,4]{1,2,0:T(4,128)} %param.13) | data formatting | bytes 8192 | tf_op args[4]
  2.1 0.0 copy-done.3
  2.1 0.8 %copy.14.gate_ref = f32[2,128,4]{2,1,0:T(8,128)} copy(f32[2,128,4]{1,2,0:T(4,128)S(1)} %copy-done.3) | data formatting | bytes 8192 | tf_op args[5]
  2.9 41.6 %shard_map.120 = (f32[128,256]{1,0:T(8,128)}, f32[128,128]{1,0:T(8,128)}, f32[128,128]{1,0:T(8,128)}, f32[256,256]{1,0:T(8,128)}) custom-call(bf16[128,256]{1,0:T(8,128)(2,1)} %q_ref.1, bf16[128,128]{1,0:T(8,128)(2,1)} %k_ref.1, bf16[128,128]{1,0:T(8,128)(2,1)} %v_ref.1, bf16[128,2048]{1,0:T(8,128)(2,1)} %hid_ref.1, f32[2,128,4]{2,1,0:T(8,128)} %copy.13.log_ref, ...), custom_call_target="tpu_custom_call" | custom-call | tf_op jit(solution)/shard_map/pallas_call | solution.py:371
  44.5 0.0 copy-start.2
  44.5 0.0 copy-start
  44.5 1.6 %copy.19 = f32[128,256]{1,0:T(8,128)} copy(f32[128,256]{1,0:T(8,128)} %get-tuple-element.8) | data formatting | bytes 262144
  46.1 0.0 copy-done.2
  46.1 0.0 copy-start.1
  46.1 0.6 %copy.20 = f32[128,128]{1,0:T(8,128)} copy(f32[128,128]{1,0:T(8,128)S(1)} %copy-done.2) | data formatting | bytes 131072
  46.8 0.2 copy-done.1
  47.0 0.6 %copy.21 = f32[128,128]{1,0:T(8,128)} copy(f32[128,128]{1,0:T(8,128)S(1)} %copy-done.1) | data formatting | bytes 131072
  47.6 0.0 copy-done
  47.6 0.7 %copy.22 = f32[256,256]{1,0:T(8,128)} copy(f32[256,256]{1,0:T(8,128)S(1)} %copy-done) | data formatting | bytes 524288
Async XLA Ops:
  0.6 1.5 %copy-start.3 = (f32[2,128,4]{1,2,0:T(4,128)S(1)}, f32[2,128,4]{1,2,0:T(4,128)}, u32[]{:S(2)}) copy-start(f32[2,128,4]{1,2,0:T(4,128)} %param.14) | copy-start | bytes 12292
  44.5 1.6 %copy-start.2 = (f32[128,128]{1,0:T(8,128)S(1)}, f32[128,128]{1,0:T(8,128)}, u32[]{:S(2)}) copy-start(f32[128,128]{1,0:T(8,128)} %get-tuple-element.9) | copy-start | bytes 196612
  44.5 3.1 %copy-start = (f32[256,256]{1,0:T(8,128)S(1)}, f32[256,256]{1,0:T(8,128)}, u32[]{:S(2)}) copy-start(f32[256,256]{1,0:T(8,128)} %get-tuple-element.11) | copy-start | bytes 786436
  46.1 0.9 %copy-start.1 = (f32[128,128]{1,0:T(8,128)S(1)}, f32[128,128]{1,0:T(8,128)}, u32[]{:S(2)}) copy-start(f32[128,128]{1,0:T(8,128)} %get-tuple-element.10) | copy-start | bytes 196612

commit v2 on v1

--- a/solution.py
+++ b/solution.py
@@ -161,10 +161,11 @@
 
 
 def fused_kernel(
-    n, q_ref, k_ref, v_ref, hid_ref, log_ref, gate_ref, out_ref, cot_ref, chosen_ref,
+    n, tps, q_ref, k_ref, v_ref, hid_ref, log_ref, gate_ref, out_ref, cot_ref, chosen_ref,
     gq_ref, gk_ref, gv_ref, gw_ref,
     table, blk_out, blk_in, grd_out, grd_in, qb_out, qb_in, hid_in, hid_t,
-    blk_send, blk_recv, hid_send, hid_recv, qb_send, qb_recv, grd_send, grd_recv, own_sem,
+    blk_send, blk_recv, hid_send, hid_recv, qb_send, qb_recv, grd_send, grd_recv,
+    pass_send, pass_recv, share_send, share_recv, own_sem,
 ):
     rows, width = q_ref.shape
     heads = width // DH
@@ -173,29 +174,38 @@
     group_heads = heads // groups
     per_block = rows // BLK
     per_summary = rows // CMP
-    pad = blk_in.shape[1] // 2 - BLK
+    pad = (blk_in.shape[1] - 2 * BLK) // 2
     qrows = rows // SUB
     cols = hid_in.shape[2]
+    part = rows // tps
     scale = DH ** (-0.5)
     me = lax.axis_index("kv")
-    to = [lax.rem(me + s, n) for s in range(n)]
-
-    def copy(src, dst, send, recv, peer):
+    my_tp = lax.axis_index("tp")
+    half = n // 2
+    place, side = me // 2, me % 2
+    to = [2 * lax.rem(place + s // 2, half) + lax.rem(side + s % 2, 2) for s in range(n)]
+    come = [2 * lax.rem(place + half - s // 2, half) + lax.rem(side + s % 2, 2) for s in range(n)]
+    mesh_id = pl.DeviceIdType.MESH
+
+    def copy(src, dst, send, recv, **peer):
         return pltpu.make_async_remote_copy(
             src_ref=src, dst_ref=dst, send_sem=send, recv_sem=recv,
-            device_id={"kv": peer}, device_id_type=pl.DeviceIdType.MESH,
+            device_id=peer, device_id_type=mesh_id,
         )
 
     barrier = pltpu.get_barrier_semaphore()
-    for s in range(1, n):
-        pl.semaphore_signal(
-            barrier, inc=1, device_id={"kv": to[s]}, device_id_type=pl.DeviceIdType.MESH
-        )
+    for s in range(n - 1, 0, -1):
+        pl.semaphore_signal(barrier, inc=1, device_id={"kv": to[s]}, device_id_type=mesh_id)
+    tp_to = [lax.rem(my_tp + u, tps) for u in range(tps)]
+    for u in range(1, tps):
+        pl.semaphore_signal(barrier, inc=1, device_id={"tp": tp_to[u]}, device_id_type=mesh_id)
+
+    part_rows = pl.ds(pl.multiple_of(my_tp * part, part), part)
 
     def hidden_of(peer):
-        return hid_ref.at[:, pl.ds(pl.multiple_of(peer * cols, cols), cols)]
-
-    own_hidden = pltpu.make_async_copy(hidden_of(me), hid_in.at[0], own_sem)
+        return hid_ref.at[part_rows, pl.ds(pl.multiple_of(peer * cols, cols), cols)]
+
+    own_hidden = pltpu.make_async_copy(hidden_of(me), hid_in.at[0, part_rows], own_sem)
     own_hidden.start()
 
     lane_group = lax.broadcasted_iota(jnp.int32, (n, lanes), 1) // DH
@@ -217,7 +227,7 @@
         for j in range(per_summary):
             mean = jnp.sum(array[j * CMP : (j + 1) * CMP], 0, keepdims=True) / CMP
             result = jnp.where(row == j, mean, result)
-        return result.astype(LOW)
+        return result
 
     def block_of(array, row):
         result = array[:BLK]
@@ -225,43 +235,49 @@
             result = jnp.where(row == b, array[b * BLK : (b + 1) * BLK], result)
         return result.astype(LOW)
 
-    sum_keys = summary_of(keys)
-    sum_values = summary_of(values)
+    sums = jnp.concatenate([summary_of(keys), summary_of(values)], 0).astype(LOW)
     for s in range(n):
         target = blk_in if s == 0 else blk_out
         target[s, :BLK] = block_of(keys, want[s])
         target[s, BLK : 2 * BLK] = block_of(values, want[s])
-        target[s, 2 * BLK : 2 * BLK + pad] = sum_keys
-        target[s, 2 * BLK + pad :] = sum_values
-
-    pl.semaphore_wait(barrier, n - 1)
+        target[s, 2 * BLK :] = sums
+
+    pl.semaphore_wait(barrier, n - 1 + tps - 1)
     blk = [
-        copy(blk_out.at[s], blk_in.at[s], blk_send.at[s], blk_recv.at[s], to[s]) for s in range(1, n)
+        copy(blk_out.at[s], blk_in.at[s], blk_send.at[s], blk_recv.at[s], kv=to[s]) for s in range(1, n)
     ]
     for c in blk:
         c.start()
     hid = [
-        copy(hidden_of(to[s]), hid_in.at[s], hid_send.at[s], hid_recv.at[s], to[s])
+        copy(hidden_of(to[s]), hid_in.at[s, part_rows], hid_send.at[s], hid_recv.at[s], kv=to[s])
         for s in range(1, n)
     ]
     for c in hid:
         c.start()
 
+    columns = jnp.concatenate([log_ref[0], log_ref[1], gate_ref[0], gate_ref[1]], 0).T
+
+    def column(kind, branch, h, count):
+        at = (2 * kind + branch) * heads + h
+        return columns[:count, at : at + 1]
+
     def head_stats(branch, h, count):
         at = slice(h * DH, (h + 1) * DH)
-        gated = gate_ref[branch, :count, h : h + 1] * cot_ref[:count, at].astype(WIDE)
+        gated = column(1, branch, h, count) * cot_ref[:count, at].astype(WIDE)
         delta = jnp.sum(gated * out_ref[branch, :count, at].astype(WIDE), -1, keepdims=True)
-        return gated.astype(LOW), delta, log_ref[branch, :count, h : h + 1], q_ref[:count, at]
+        return gated.astype(LOW), delta, column(0, branch, h, count), q_ref[:count, at]
 
     def stats(branch, g, count):
         each = [head_stats(branch, g * group_heads + r, count) for r in range(group_heads)]
-        return [jnp.concatenate(part, 0) for part in zip(*each)]
+        return [jnp.concatenate(piece, 0) for piece in zip(*each)]
 
     prepared = [(stats(0, g, rows), stats(1, g, qrows)) for g in range(groups)]
 
     def owner_of(shape, per_slot):
-        slot = lax.broadcasted_iota(jnp.int32, shape, 1)
-        return lax.rem(me - slot // per_slot + n, n), slot % per_slot
+        column_at = lax.broadcasted_iota(jnp.int32, shape, 1)
+        slot = column_at // per_slot
+        owner = 2 * lax.rem(place + half - slot // 2, half) + lax.rem(side + slot % 2, 2)
+        return owner, column_at % per_slot
 
     shape0 = (group_heads * rows, n * pad)
     owner0, inner0 = owner_of(shape0, pad)
@@ -280,9 +296,10 @@
         c.wait_recv()
     all_keys = blk_in[:, :BLK].reshape(n * BLK, lanes)
     all_values = blk_in[:, BLK : 2 * BLK].reshape(n * BLK, lanes)
-    all_sum_keys = blk_in[:, 2 * BLK : 2 * BLK + pad].reshape(n * pad, lanes)
-    all_sum_values = blk_in[:, 2 * BLK + pad :].reshape(n * pad, lanes)
-    probs_all, score_all, grads = [], [], []
+    all_sums = blk_in[:, 2 * BLK :].astype(WIDE)
+    all_sum_keys = all_sums[:, :pad].reshape(n * pad, lanes).astype(LOW)
+    all_sum_values = all_sums[:, pad:].reshape(n * pad, lanes).astype(LOW)
+    probs_all, score_all = [], []
     for g in range(groups):
         at = slice(g * DH, (g + 1) * DH)
         (low0, delta0, log0, query0), (low1, delta1, log1, query1) = prepared[g]
@@ -302,7 +319,16 @@
         probs_all.append((probs0, probs1))
         score_all.append((score0, score1))
     qb_out[...] = gq_ref[...].astype(LOW)
-    qb = [copy(qb_out, qb_in.at[s], qb_send.at[s], qb_recv.at[s], to[s]) for s in range(1, n)]
+    direct = [s for s in range(1, n) if s % 2 == 0 or s == 1]
+    qb = {
+        s: copy(qb_out, qb_in.at[s], qb_send.at[s], qb_recv.at[s], kv=to[s]) for s in direct
+    }
+    passed = {
+        s: copy(qb_in.at[s], qb_in.at[s + 1], pass_send.at[s], pass_recv.at[s], kv=to[1])
+        for s in range(2, n, 2)
+    }
+    for s in reversed(direct):
+        qb[s].start()
 
     def wide_of(parts):
         return jnp.concatenate(parts, 1)
@@ -314,35 +340,40 @@
     for s in range(1, n):
         grd_out[s, :BLK] = key1[s * BLK : (s + 1) * BLK].astype(LOW)
         grd_out[s, BLK : 2 * BLK] = value1[s * BLK : (s + 1) * BLK].astype(LOW)
-        grd_out[s, 2 * BLK : 2 * BLK + pad] = key0[s * pad : (s + 1) * pad].astype(LOW)
-        grd_out[s, 2 * BLK + pad :] = value0[s * pad : (s + 1) * pad].astype(LOW)
+        both = [key0[s * pad : (s + 1) * pad], value0[s * pad : (s + 1) * pad]]
+        grd_out[s, 2 * BLK :] = jnp.concatenate(both, 0).astype(LOW)
     grd = [
-        copy(grd_out.at[s], grd_in.at[s], grd_send.at[s], grd_recv.at[s], to[n - s])
+        copy(grd_out.at[s], grd_in.at[s], grd_send.at[s], grd_recv.at[s], kv=come[s])
         for s in range(1, n)
     ]
-    for c in qb:
-        c.start()
     for c in grd:
         c.start()
 
     own_hidden.wait()
-    hid_t[0] = hid_in[0].T
-    total = dot(hid_t[0], qb_out[...], NN)
-    for s in range(1, n):
-        hid[s - 1].wait_recv()
-        hid_t[s] = hid_in[s].T
+    for c in hid:
+        c.wait_recv()
+    mine = hid_in.at[:, part_rows]
+    share = [
+        copy(mine, mine, share_send.at[u], share_recv.at[u], tp=tp_to[u]) for u in range(1, tps)
+    ]
+    for c in share:
+        c.start()
+
+    for s in range(2, n, 2):
+        qb[s].wait_recv()
+        passed[s].start()
 
     for c in grd:
         c.wait_recv()
     for block_part, sum_part, own_block, own_sum, result in (
-        (0, 2 * BLK, key1, key0, gk_ref),
-        (BLK, 2 * BLK + pad, value1, value0, gv_ref),
+        (0, 0, key1, key0, gk_ref),
+        (BLK, pad, value1, value0, gv_ref),
     ):
         here = [own_block[:BLK]]
         summed = own_sum[:pad]
         for s in range(1, n):
             here.append(grd_in[s, block_part : block_part + BLK].astype(WIDE))
-            summed = summed + grd_in[s, sum_part : sum_part + pad].astype(WIDE)
+            summed = summed + grd_in[s, 2 * BLK :].astype(WIDE)[sum_part : sum_part + pad]
         for b in range(per_block):
             block = jnp.zeros((BLK, lanes), WIDE)
             for s in range(n):
@@ -352,24 +383,36 @@
                 term = summed[at // CMP : at // CMP + 1] / CMP
                 result[at : at + CMP] = block[j * CMP : (j + 1) * CMP] + term
 
-    for s in range(1, n):
-        qb[s - 1].wait_recv()
+    for u in range(1, tps):
+        other = lax.rem(my_tp + tps - u, tps)
+        arrived = hid_in.at[:, pl.ds(pl.multiple_of(other * part, part), part)]
+        copy(mine, arrived, share_send.at[u], share_recv.at[u], tp=tp_to[u]).wait_recv()
+    for s in range(n):
+        hid_t[s] = hid_in[s].T
+    total = dot(hid_t[0], qb_out[...], NN)
+    for s in range(2, n, 2):
         total = total + dot(hid_t[s], qb_in[s], NN)
+    qb[1].wait_recv()
+    total = total + dot(hid_t[1], qb_in[1], NN)
+    for s in range(2, n, 2):
+        passed[s].wait_recv()
+        total = total + dot(hid_t[s + 1], qb_in[s + 1], NN)
     gw_ref[...] = total
-    for c in blk + hid + qb + grd:
+    for c in blk + hid + list(qb.values()) + grd + share + list(passed.values()):
         c.wait_send()
 
 
-def fused(n, queries, keys, values, hidden, log_sums, gates, branch_out, cotangent, chosen):
+def fused(n, tps, queries, keys, values, hidden, log_sums, gates, branch_out, cotangent, chosen):
     rows, width = queries.shape
     lanes = keys.shape[1]
     cols = hidden.shape[1] // n
-    pad = -(-(rows // CMP) // 16) * 16
+    pad = -(-(rows // CMP) // 8) * 8
     size = 2 * (BLK + pad)
     vmem = pl.BlockSpec(memory_space=pltpu.VMEM)
     sems = pltpu.SemaphoreType.DMA((n,))
+    tp_sems = pltpu.SemaphoreType.DMA((tps,))
     return pl.pallas_call(
-        functools.partial(fused_kernel, n),
+        functools.partial(fused_kernel, n, tps),
         out_shape=(
             jax.ShapeDtypeStruct((rows, width), WIDE),
             jax.ShapeDtypeStruct((rows, lanes), WIDE),
@@ -388,23 +431,28 @@
             pltpu.VMEM((n, rows, width), LOW),
             pltpu.VMEM((n, rows, cols), LOW),
             pltpu.VMEM((n, cols, rows), LOW),
-            sems, sems, sems, sems, sems, sems, sems, sems,
+            sems, sems, sems, sems, sems, sems, sems, sems, sems, sems,
+            tp_sems, tp_sems,
             pltpu.SemaphoreType.DMA,
         ],
         compiler_params=pltpu.CompilerParams(collective_id=0, has_side_effects=True),
-    )(queries, keys, values, hidden, log_sums, gates, branch_out, cotangent, chosen)
-
-
-def fits(n, hidden, chosen):
-    return chosen.shape[0] <= TOPN and (hidden.shape[1] // n) % 128 == 0
+    )(
+        queries, keys, values, hidden, jnp.swapaxes(log_sums, 1, 2), jnp.swapaxes(gates, 1, 2),
+        branch_out, cotangent, chosen,
+    )
+
+
+def fits(n, tps, hidden, chosen):
+    whole = (hidden.shape[1] // n) % 128 == 0 and (hidden.shape[0] // tps) % 16 == 0
+    return chosen.shape[0] <= TOPN and n % 2 == 0 and whole
 
 
 def solution(mesh):
 
-    n = mesh.shape["kv"]
+    n, tps = mesh.shape["kv"], mesh.shape["tp"]
 
     def body(*args):
-        return fused(n, *args) if fits(n, args[3], args[8]) else shards(*args)
+        return fused(n, tps, *args) if fits(n, tps, args[3], args[8]) else shards(*args)
 
     return jax.shard_map(
         body,

time: 48.6 us -> 33.8 us (0.70)
  Pallas kernels: 41.6 us -> 29.1 us
  local copies, waits for them, and re-layouts: 6.11 us -> 3.82 us
    pallas_call x1, Pallas kernels: 41.6 us -> 29.1 us  [fused(): pl.pallas_call(functools.partial(fused_kernel, n, tps), out_shape=(jax.Sh...]
    unnamed x14 -> x10, local copies, waits for them, and re-layouts: 6.11 us -> 3.82 us
where the time goes in v2:
time: 33.8 us; the launch traced here: 33.6 us
  Pallas kernels  29.1 us (86%)
  local copies, waits for them, and re-layouts  3.82 us (11%)
  between operations  0.66 us (2%)
    pallas_call x1, Pallas kernels, fused(): pl.pallas_call(functools.partial(fused_kernel, n, tps), out_shape=(jax.Sh...  29.1 us
    unnamed x10, local copies, waits for them, and re-layouts  3.82 us

profile of v2, /device:TPU:0, one launch (start us, length us, event | category | flops | bytes accessed | tf_op | source)
XLA Modules:
  0.0 33.6 jit_solution(3033830606118475641)
XLA Ops:
  0.6 29.1 %shard_map.120 = (f32[128,256]{1,0:T(8,128)}, f32[128,128]{1,0:T(8,128)}, f32[128,128]{1,0:T(8,128)}, f32[256,256]{1,0:T(8,128)}) custom-call(bf16[128,256]{1,0:T(8,128)(2,1)} %q_ref.1, bf16[128,128]{1,0:T(8,128)(2,1)} %k_ref.1, bf16[128,128]{1,0:T(8,128)(2,1)} %v_ref.1, bf16[128,2048]{1,0:T(8,128)(2,1)} %hid_ref.1, f32[2,4,128]{2,1,0:T(4,128)} %bitcast.2, ...), custom_call_target="tpu_custom_call" | custom-call | tf_op jit(solution)/shard_map/pallas_call | solution.py:414
  29.7 0.0 copy-start.2
  29.7 0.0 copy-start
  29.7 1.6 %copy.17 = f32[128,256]{1,0:T(8,128)} copy(f32[128,256]{1,0:T(8,128)} %get-tuple-element.8) | data formatting | bytes 262144
  31.4 0.0 copy-done.2
  31.4 0.0 copy-start.1
  31.4 0.6 %copy.18 = f32[128,128]{1,0:T(8,128)} copy(f32[128,128]{1,0:T(8,128)S(1)} %copy-done.2) | data formatting | bytes 131072
  32.0 0.2 copy-done.1
  32.2 0.6 %copy.19 = f32[128,128]{1,0:T(8,128)} copy(f32[128,128]{1,0:T(8,128)S(1)} %copy-done.1) | data formatting | bytes 131072
  32.8 0.0 copy-done
  32.8 0.7 %copy.20 = f32[256,256]{1,0:T(8,128)} copy(f32[256,256]{1,0:T(8,128)S(1)} %copy-done) | data formatting | bytes 524288
Async XLA Ops:
  29.7 1.6 %copy-start.2 = (f32[128,128]{1,0:T(8,128)S(1)}, f32[128,128]{1,0:T(8,128)}, u32[]{:S(2)}) copy-start(f32[128,128]{1,0:T(8,128)} %get-tuple-element.9) | copy-start | bytes 196612
  29.7 3.1 %copy-start = (f32[256,256]{1,0:T(8,128)S(1)}, f32[256,256]{1,0:T(8,128)}, u32[]{:S(2)}) copy-start(f32[256,256]{1,0:T(8,128)} %get-tuple-element.11) | copy-start | bytes 786436
  31.4 0.9 %copy-start.1 = (f32[128,128]{1,0:T(8,128)S(1)}, f32[128,128]{1,0:T(8,128)}, u32[]{:S(2)}) copy-start(f32[128,128]{1,0:T(8,128)} %get-tuple-element.10) | copy-start | bytes 196612

commit v3 on v2

--- a/solution.py
+++ b/solution.py
@@ -161,11 +161,12 @@
 
 
 def fused_kernel(
-    n, tps, q_ref, k_ref, v_ref, hid_ref, log_ref, gate_ref, out_ref, cot_ref, chosen_ref,
+    n, tps, q_hbm, k_hbm, v_hbm, hid_ref, log_hbm, gate_hbm, out_hbm, cot_hbm, chosen_hbm,
     gq_ref, gk_ref, gv_ref, gw_ref,
-    table, blk_out, blk_in, grd_out, grd_in, qb_out, qb_in, hid_in, hid_t,
-    blk_send, blk_recv, hid_send, hid_recv, qb_send, qb_recv, grd_send, grd_recv,
-    pass_send, pass_recv, share_send, share_recv, own_sem,
+    k_ref, v_ref, chosen_ref, q_ref, cot_ref, gate_ref, out_ref, log_ref,
+    table, sum_out, sum_in, blk_out, blk_in, grd_out, grd_in, qb_out, qb_in, hid_in, hid_t,
+    sum_send, sum_recv, blk_send, blk_recv, hid_send, hid_recv, qb_send, qb_recv,
+    grd_send, grd_recv, pass_send, pass_recv, share_send, share_recv, own_sem, load_sem,
 ):
     rows, width = q_ref.shape
     heads = width // DH
@@ -174,7 +175,7 @@
     group_heads = heads // groups
     per_block = rows // BLK
     per_summary = rows // CMP
-    pad = (blk_in.shape[1] - 2 * BLK) // 2
+    pad = sum_in.shape[1] // 2
     qrows = rows // SUB
     cols = hid_in.shape[2]
     part = rows // tps
@@ -193,6 +194,11 @@
             device_id=peer, device_id_type=mesh_id,
         )
 
+    pairs = (
+        (k_hbm, k_ref), (v_hbm, v_ref), (chosen_hbm, chosen_ref), (q_hbm, q_ref),
+        (cot_hbm, cot_ref), (gate_hbm, gate_ref), (out_hbm, out_ref), (log_hbm, log_ref),
+    )
+    loads = [pltpu.make_async_copy(*pair, load_sem.at[i]) for i, pair in enumerate(pairs)]
     barrier = pltpu.get_barrier_semaphore()
     for s in range(n - 1, 0, -1):
         pl.semaphore_signal(barrier, inc=1, device_id={"kv": to[s]}, device_id_type=mesh_id)
@@ -200,6 +206,25 @@
     for u in range(1, tps):
         pl.semaphore_signal(barrier, inc=1, device_id={"tp": tp_to[u]}, device_id_type=mesh_id)
 
+    for c in loads:
+        c.start()
+    later = [to[s] > me for s in range(n)]
+    earlier = [come[s] < me for s in range(n)]
+
+    def each(copies, conditions, act):
+        for c, condition in zip(copies, conditions[1:]):
+            pl.when(condition)(functools.partial(act, c))
+
+    for s in range(1, n):
+
+        @pl.when(jnp.logical_not(earlier[s]))
+        def _():
+            blk_in[s] = jnp.zeros(blk_in.shape[1:], LOW)
+
+        @pl.when(jnp.logical_not(later[s]))
+        def _():
+            grd_in[s] = jnp.zeros(grd_in.shape[1:], LOW)
+
     part_rows = pl.ds(pl.multiple_of(my_tp * part, part), part)
 
     def hidden_of(peer):
@@ -208,6 +233,8 @@
     own_hidden = pltpu.make_async_copy(hidden_of(me), hid_in.at[0, part_rows], own_sem)
     own_hidden.start()
 
+    for c in loads[:3]:
+        c.wait()
     lane_group = lax.broadcasted_iota(jnp.int32, (n, lanes), 1) // DH
     wanted = jnp.zeros((n, lanes), WIDE)
     for g in range(groups):
@@ -235,19 +262,23 @@
             result = jnp.where(row == b, array[b * BLK : (b + 1) * BLK], result)
         return result.astype(LOW)
 
-    sums = jnp.concatenate([summary_of(keys), summary_of(values)], 0).astype(LOW)
+    sum_out[...] = jnp.concatenate([summary_of(keys), summary_of(values)], 0).astype(LOW)
+    sum_in[0] = sum_out[...]
     for s in range(n):
         target = blk_in if s == 0 else blk_out
         target[s, :BLK] = block_of(keys, want[s])
         target[s, BLK : 2 * BLK] = block_of(values, want[s])
-        target[s, 2 * BLK :] = sums
 
     pl.semaphore_wait(barrier, n - 1 + tps - 1)
     blk = [
         copy(blk_out.at[s], blk_in.at[s], blk_send.at[s], blk_recv.at[s], kv=to[s]) for s in range(1, n)
     ]
-    for c in blk:
+    summed_in = [
+        copy(sum_out, sum_in.at[s], sum_send.at[s], sum_recv.at[s], kv=to[s]) for s in range(1, n)
+    ]
+    for c in summed_in:
         c.start()
+    each(blk, later, lambda c: c.start())
     hid = [
         copy(hidden_of(to[s]), hid_in.at[s, part_rows], hid_send.at[s], hid_recv.at[s], kv=to[s])
         for s in range(1, n)
@@ -255,6 +286,8 @@
     for c in hid:
         c.start()
 
+    for c in loads[3:]:
+        c.wait()
     columns = jnp.concatenate([log_ref[0], log_ref[1], gate_ref[0], gate_ref[1]], 0).T
 
     def column(kind, branch, h, count):
@@ -268,8 +301,8 @@
         return gated.astype(LOW), delta, column(0, branch, h, count), q_ref[:count, at]
 
     def stats(branch, g, count):
-        each = [head_stats(branch, g * group_heads + r, count) for r in range(group_heads)]
-        return [jnp.concatenate(piece, 0) for piece in zip(*each)]
+        found = [head_stats(branch, g * group_heads + r, count) for r in range(group_heads)]
+        return [jnp.concatenate(piece, 0) for piece in zip(*found)]
 
     prepared = [(stats(0, g, rows), stats(1, g, qrows)) for g in range(groups)]
 
@@ -292,51 +325,73 @@
         score = (probs * (dot(low, value, NT) - delta)).astype(LOW)
         return probs.astype(LOW), score
 
-    for c in blk:
+    for c in summed_in:
         c.wait_recv()
-    all_keys = blk_in[:, :BLK].reshape(n * BLK, lanes)
-    all_values = blk_in[:, BLK : 2 * BLK].reshape(n * BLK, lanes)
-    all_sums = blk_in[:, 2 * BLK :].astype(WIDE)
+    all_sums = sum_in[...].astype(WIDE)
     all_sum_keys = all_sums[:, :pad].reshape(n * pad, lanes).astype(LOW)
     all_sum_values = all_sums[:, pad:].reshape(n * pad, lanes).astype(LOW)
-    probs_all, score_all = [], []
+
+    def wide_of(parts):
+        return jnp.concatenate(parts, 1)
+
+    grad0, key0, value0 = [], [], []
     for g in range(groups):
         at = slice(g * DH, (g + 1) * DH)
-        (low0, delta0, log0, query0), (low1, delta1, log1, query1) = prepared[g]
+        low0, delta0, log0, query0 = prepared[g][0]
+        probs0, score0 = branch(query0, all_sum_keys[:, at], all_sum_values[:, at], seen0, low0, delta0, log0)
+        grad0.append(dot(score0, all_sum_keys[:, at], NN) * scale)
+        for r in range(group_heads):
+            h = slice((g * group_heads + r) * DH, (g * group_heads + r + 1) * DH)
+            gq_ref[qrows:, h] = grad0[g][r * rows + qrows : (r + 1) * rows]
+        key0.append((score0, query0))
+        value0.append((probs0, low0))
+    direct = [s for s in range(1, n) if s % 2 == 0 or s == 1]
+    pieces = (slice(qrows, rows), slice(0, qrows))
+    qb = [
+        {
+            s: copy(qb_out.at[piece], qb_in.at[s, piece], qb_send.at[i, s], qb_recv.at[i, s], kv=to[s])
+            for s in direct
+        }
+        for i, piece in enumerate(pieces)
+    ]
+    passed = [
+        {
+            s: copy(
+                qb_in.at[s, piece], qb_in.at[s + 1, piece],
+                pass_send.at[i, s], pass_recv.at[i, s], kv=to[1],
+            )
+            for s in range(2, n, 2)
+        }
+        for i, piece in enumerate(pieces)
+    ]
+    qb_out[qrows:] = gq_ref[qrows:].astype(LOW)
+    for s in reversed(direct):
+        qb[0][s].start()
+    key0 = wide_of([dot(score, query, TN) for score, query in key0]) * scale
+    value0 = wide_of([dot(probs, low, TN) for probs, low in value0])
+
+    each(blk, earlier, lambda c: c.wait_recv())
+    all_keys = blk_in[:, :BLK].reshape(n * BLK, lanes)
+    all_values = blk_in[:, BLK:].reshape(n * BLK, lanes)
+    key1, value1 = [], []
+    for g in range(groups):
+        at = slice(g * DH, (g + 1) * DH)
+        low1, delta1, log1, query1 = prepared[g][1]
         own_block = want[0][:, g * DH : g * DH + 1]
         first = own_block * BLK + inner1.astype(WIDE) <= time1.astype(WIDE)
         seen1 = (owner1 < me) | ((owner1 == me) & first)
-        probs0, score0 = branch(query0, all_sum_keys[:, at], all_sum_values[:, at], seen0, low0, delta0, log0)
         probs1, score1 = branch(query1, all_keys[:, at], all_values[:, at], seen1, low1, delta1, log1)
-        grad0 = dot(score0, all_sum_keys[:, at], NN) * scale
         grad1 = dot(score1, all_keys[:, at], NN) * scale
         for r in range(group_heads):
             h = slice((g * group_heads + r) * DH, (g * group_heads + r + 1) * DH)
-            start = r * rows
-            top = grad0[start : start + qrows] + grad1[r * qrows : (r + 1) * qrows]
-            gq_ref[:qrows, h] = top
-            gq_ref[qrows:, h] = grad0[start + qrows : start + rows]
-        probs_all.append((probs0, probs1))
-        score_all.append((score0, score1))
-    qb_out[...] = gq_ref[...].astype(LOW)
-    direct = [s for s in range(1, n) if s % 2 == 0 or s == 1]
-    qb = {
-        s: copy(qb_out, qb_in.at[s], qb_send.at[s], qb_recv.at[s], kv=to[s]) for s in direct
-    }
-    passed = {
-        s: copy(qb_in.at[s], qb_in.at[s + 1], pass_send.at[s], pass_recv.at[s], kv=to[1])
-        for s in range(2, n, 2)
-    }
+            gq_ref[:qrows, h] = grad0[g][r * rows : r * rows + qrows] + grad1[r * qrows : (r + 1) * qrows]
+        key1.append((score1, query1))
+        value1.append((probs1, low1))
+    qb_out[:qrows] = gq_ref[:qrows].astype(LOW)
     for s in reversed(direct):
-        qb[s].start()
-
-    def wide_of(parts):
-        return jnp.concatenate(parts, 1)
-
-    key1 = wide_of([dot(score_all[g][1], prepared[g][1][3], TN) for g in range(groups)]) * scale
-    value1 = wide_of([dot(probs_all[g][1], prepared[g][1][0], TN) for g in range(groups)])
-    key0 = wide_of([dot(score_all[g][0], prepared[g][0][3], TN) for g in range(groups)]) * scale
-    value0 = wide_of([dot(probs_all[g][0], prepared[g][0][0], TN) for g in range(groups)])
+        qb[1][s].start()
+    key1 = wide_of([dot(score, query, TN) for score, query in key1]) * scale
+    value1 = wide_of([dot(probs, low, TN) for probs, low in value1])
     for s in range(1, n):
         grd_out[s, :BLK] = key1[s * BLK : (s + 1) * BLK].astype(LOW)
         grd_out[s, BLK : 2 * BLK] = value1[s * BLK : (s + 1) * BLK].astype(LOW)
@@ -346,8 +401,7 @@
         copy(grd_out.at[s], grd_in.at[s], grd_send.at[s], grd_recv.at[s], kv=come[s])
         for s in range(1, n)
     ]
-    for c in grd:
-        c.start()
+    each(grd, earlier, lambda c: c.start())
 
     own_hidden.wait()
     for c in hid:
@@ -359,12 +413,25 @@
     for c in share:
         c.start()
 
+    for i in range(len(pieces)):
+        for s in range(2, n, 2):
+            qb[i][s].wait_recv()
+            passed[i][s].start()
+
+    for u in range(1, tps):
+        other = lax.rem(my_tp + tps - u, tps)
+        arrived = hid_in.at[:, pl.ds(pl.multiple_of(other * part, part), part)]
+        copy(mine, arrived, share_send.at[u], share_recv.at[u], tp=tp_to[u]).wait_recv()
+    for s in range(n):
+        hid_t[s] = hid_in[s].T
+    total = dot(hid_t[0], qb_out[...], NN)
     for s in range(2, n, 2):
-        qb[s].wait_recv()
-        passed[s].start()
-
-    for c in grd:
-        c.wait_recv()
+        total = total + dot(hid_t[s], qb_in[s], NN)
+    for i in range(len(pieces)):
+        qb[i][1].wait_recv()
+    total = total + dot(hid_t[1], qb_in[1], NN)
+
+    each(grd, later, lambda c: c.wait_recv())
     for block_part, sum_part, own_block, own_sum, result in (
         (0, 0, key1, key0, gk_ref),
         (BLK, pad, value1, value0, gv_ref),
@@ -383,23 +450,18 @@
                 term = summed[at // CMP : at // CMP + 1] / CMP
                 result[at : at + CMP] = block[j * CMP : (j + 1) * CMP] + term
 
-    for u in range(1, tps):
-        other = lax.rem(my_tp + tps - u, tps)
-        arrived = hid_in.at[:, pl.ds(pl.multiple_of(other * part, part), part)]
-        copy(mine, arrived, share_send.at[u], share_recv.at[u], tp=tp_to[u]).wait_recv()
-    for s in range(n):
-        hid_t[s] = hid_in[s].T
-    total = dot(hid_t[0], qb_out[...], NN)
     for s in range(2, n, 2):
-        total = total + dot(hid_t[s], qb_in[s], NN)
-    qb[1].wait_recv()
-    total = total + dot(hid_t[1], qb_in[1], NN)
-    for s in range(2, n, 2):
-        passed[s].wait_recv()
+        for i in range(len(pieces)):
+            passed[i][s].wait_recv()
         total = total + dot(hid_t[s + 1], qb_in[s + 1], NN)
     gw_ref[...] = total
-    for c in blk + hid + list(qb.values()) + grd + share + list(passed.values()):
+    for c in summed_in + hid + share:
         c.wait_send()
+    for i in range(len(pieces)):
+        for c in list(qb[i].values()) + list(passed[i].values()):
+            c.wait_send()
+    each(blk, later, lambda c: c.wait_send())
+    each(grd, earlier, lambda c: c.wait_send())
 
 
 def fused(n, tps, queries, keys, values, hidden, log_sums, gates, branch_out, cotangent, chosen):
@@ -407,9 +469,11 @@
     lanes = keys.shape[1]
     cols = hidden.shape[1] // n
     pad = -(-(rows // CMP) // 8) * 8
-    size = 2 * (BLK + pad)
+    groups, nsel = chosen.shape[1:]
+    heads = log_sums.shape[2]
     vmem = pl.BlockSpec(memory_space=pltpu.VMEM)
     sems = pltpu.SemaphoreType.DMA((n,))
+    two_sems = pltpu.SemaphoreType.DMA((2, n))
     tp_sems = pltpu.SemaphoreType.DMA((tps,))
     return pl.pallas_call(
         functools.partial(fused_kernel, n, tps),
@@ -419,21 +483,32 @@
             jax.ShapeDtypeStruct((rows, lanes), WIDE),
             jax.ShapeDtypeStruct((cols, width), WIDE),
         ),
-        in_specs=[vmem] * 3 + [pl.BlockSpec(memory_space=pl.ANY)] + [vmem] * 5,
+        in_specs=[pl.BlockSpec(memory_space=pl.ANY)] * 9,
         out_specs=(vmem,) * 4,
         scratch_shapes=[
+            pltpu.VMEM((rows, lanes), LOW),
+            pltpu.VMEM((rows, lanes), LOW),
+            pltpu.VMEM((n, groups, nsel), jnp.int32),
+            pltpu.VMEM((rows, width), LOW),
+            pltpu.VMEM((rows, width), LOW),
+            pltpu.VMEM((2, heads, rows), WIDE),
+            pltpu.VMEM((2, rows, width), LOW),
+            pltpu.VMEM((2, heads, rows), WIDE),
             pltpu.VMEM((n, lanes), WIDE),
-            pltpu.VMEM((n, size, lanes), LOW),
-            pltpu.VMEM((n, size, lanes), LOW),
-            pltpu.VMEM((n, size, lanes), LOW),
-            pltpu.VMEM((n, size, lanes), LOW),
+            pltpu.VMEM((2 * pad, lanes), LOW),
+            pltpu.VMEM((n, 2 * pad, lanes), LOW),
+            pltpu.VMEM((n, 2 * BLK, lanes), LOW),
+            pltpu.VMEM((n, 2 * BLK, lanes), LOW),
+            pltpu.VMEM((n, 2 * BLK + 2 * pad, lanes), LOW),
+            pltpu.VMEM((n, 2 * BLK + 2 * pad, lanes), LOW),
             pltpu.VMEM((rows, width), LOW),
             pltpu.VMEM((n, rows, width), LOW),
             pltpu.VMEM((n, rows, cols), LOW),
             pltpu.VMEM((n, cols, rows), LOW),
-            sems, sems, sems, sems, sems, sems, sems, sems, sems, sems,
+            sems, sems, sems, sems, sems, sems, two_sems, two_sems, sems, sems, two_sems, two_sems,
             tp_sems, tp_sems,
             pltpu.SemaphoreType.DMA,
+            pltpu.SemaphoreType.DMA((8,)),
         ],
         compiler_params=pltpu.CompilerParams(collective_id=0, has_side_effects=True),
     )(

time: 33.8 us -> 29.7 us (0.88)
  Pallas kernels: 29.1 us -> 25 us
    pallas_call x1, Pallas kernels: 29.1 us -> 25 us  [fused(): pl.pallas_call(functools.partial(fused_kernel, n, tps), out_shape=(jax.Sh...]
where the time goes in v3:
time: 29.7 us; the launch traced here: 29.5 us
  Pallas kernels  25 us (84%)
  local copies, waits for them, and re-layouts  3.82 us (13%)
  between operations  0.66 us (2%)
    pallas_call x1, Pallas kernels, fused(): pl.pallas_call(functools.partial(fused_kernel, n, tps), out_shape=(jax.Sh...  25 us
    unnamed x10, local copies, waits for them, and re-layouts  3.82 us

profile of v3, /device:TPU:0, one launch (start us, length us, event | category | flops | bytes accessed | tf_op | source)
XLA Modules:
  0.0 29.5 jit_solution(1067713567788610920)
XLA Ops:
  0.6 25.0 %shard_map.120 = (f32[128,256]{1,0:T(8,128)}, f32[128,128]{1,0:T(8,128)}, f32[128,128]{1,0:T(8,128)}, f32[256,256]{1,0:T(8,128)}) custom-call(bf16[128,256]{1,0:T(8,128)(2,1)} %q_hbm.1, bf16[128,128]{1,0:T(8,128)(2,1)} %k_hbm.1, bf16[128,128]{1,0:T(8,128)(2,1)} %v_hbm.1, bf16[128,2048]{1,0:T(8,128)(2,1)} %hid_ref.1, f32[2,4,128]{2,1,0:T(4,128)} %bitcast.2, ...), custom_call_target="tpu_custom_call" | custom-call | tf_op jit(solution)/shard_map/pallas_call | solution.py:478
  25.6 0.0 copy-start.2
  25.6 0.0 copy-start
  25.6 1.6 %copy.17 = f32[128,256]{1,0:T(8,128)} copy(f32[128,256]{1,0:T(8,128)} %get-tuple-element.8) | data formatting | bytes 262144
  27.3 0.0 copy-done.2
  27.3 0.0 copy-start.1
  27.3 0.6 %copy.18 = f32[128,128]{1,0:T(8,128)} copy(f32[128,128]{1,0:T(8,128)S(1)} %copy-done.2) | data formatting | bytes 131072
  27.9 0.2 copy-done.1
  28.1 0.6 %copy.19 = f32[128,128]{1,0:T(8,128)} copy(f32[128,128]{1,0:T(8,128)S(1)} %copy-done.1) | data formatting | bytes 131072
  28.8 0.0 copy-done
  28.8 0.7 %copy.20 = f32[256,256]{1,0:T(8,128)} copy(f32[256,256]{1,0:T(8,128)S(1)} %copy-done) | data formatting | bytes 524288
Async XLA Ops:
  25.6 1.6 %copy-start.2 = (f32[128,128]{1,0:T(8,128)S(1)}, f32[128,128]{1,0:T(8,128)}, u32[]{:S(2)}) copy-start(f32[128,128]{1,0:T(8,128)} %get-tuple-element.9) | copy-start | bytes 196612
  25.6 3.1 %copy-start = (f32[256,256]{1,0:T(8,128)S(1)}, f32[256,256]{1,0:T(8,128)}, u32[]{:S(2)}) copy-start(f32[256,256]{1,0:T(8,128)} %get-tuple-element.11) | copy-start | bytes 786436
  27.3 0.9 %copy-start.1 = (f32[128,128]{1,0:T(8,128)S(1)}, f32[128,128]{1,0:T(8,128)}, u32[]{:S(2)}) copy-start(f32[128,128]{1,0:T(8,128)} %get-tuple-element.10) | copy-start | bytes 196612

commit v4 on v3

--- a/solution.py
+++ b/solution.py
@@ -464,6 +464,12 @@
     each(grd, earlier, lambda c: c.wait_send())
 
 
+def place_kernel(*refs):
+    count = len(refs) // 2
+    for source, target in zip(refs[:count], refs[count:]):
+        target[...] = source[...]
+
+
 def fused(n, tps, queries, keys, values, hidden, log_sums, gates, branch_out, cotangent, chosen):
     rows, width = queries.shape
     lanes = keys.shape[1]
@@ -472,17 +478,13 @@
     groups, nsel = chosen.shape[1:]
     heads = log_sums.shape[2]
     vmem = pl.BlockSpec(memory_space=pltpu.VMEM)
+    shapes = ((rows, width), (rows, lanes), (rows, lanes), (cols, width))
     sems = pltpu.SemaphoreType.DMA((n,))
     two_sems = pltpu.SemaphoreType.DMA((2, n))
     tp_sems = pltpu.SemaphoreType.DMA((tps,))
-    return pl.pallas_call(
+    results = pl.pallas_call(
         functools.partial(fused_kernel, n, tps),
-        out_shape=(
-            jax.ShapeDtypeStruct((rows, width), WIDE),
-            jax.ShapeDtypeStruct((rows, lanes), WIDE),
-            jax.ShapeDtypeStruct((rows, lanes), WIDE),
-            jax.ShapeDtypeStruct((cols, width), WIDE),
-        ),
+        out_shape=tuple(pltpu.VMEM(shape, WIDE) for shape in shapes),
         in_specs=[pl.BlockSpec(memory_space=pl.ANY)] * 9,
         out_specs=(vmem,) * 4,
         scratch_shapes=[
@@ -515,6 +517,12 @@
         queries, keys, values, hidden, jnp.swapaxes(log_sums, 1, 2), jnp.swapaxes(gates, 1, 2),
         branch_out, cotangent, chosen,
     )
+    return pl.pallas_call(
+        place_kernel,
+        out_shape=tuple(jax.ShapeDtypeStruct(shape, WIDE) for shape in shapes),
+        in_specs=[vmem] * len(shapes),
+        out_specs=(vmem,) * len(shapes),
+    )(*(pltpu.with_memory_space_constraint(result, pltpu.VMEM) for result in results))
 
 
 def fits(n, tps, hidden, chosen):

time: 29.7 us -> 25.8 us (0.87)
  local copies, waits for them, and re-layouts: 3.82 us -> 0 us
    unnamed x10 -> x0, local copies, waits for them, and re-layouts: 3.82 us -> none
    pallas_call x1 -> x2, Pallas kernels: 25 us -> 25 us  [the longest x1 24.2 us: fused(): pl.pallas_call(functools.partial(fused_kernel, n, tps), out_shape=tuple((...]
where the time goes in v4:
time: 25.8 us; the launch traced here: 25.7 us
  Pallas kernels  25 us (97%)
  between operations  0.64 us (2%)
    pallas_call x1, Pallas kernels, fused(): pl.pallas_call(functools.partial(fused_kernel, n, tps), out_shape=tuple((...  24.2 us
    pallas_call x1, Pallas kernels, fused(): pl.pallas_call(place_kernel, out_shape=tuple((jax.ShapeDtypeStruct(shape,...  0.82 us

profile of v4, /device:TPU:0, one launch (start us, length us, event | category | flops | bytes accessed | tf_op | source)
XLA Modules:
  0.0 25.7 jit_solution(10981767700577435853)
XLA Ops:
  0.6 24.2 %shard_map.120 = (f32[128,256]{1,0:T(8,128)S(1)}, f32[128,128]{1,0:T(8,128)S(1)}, f32[128,128]{1,0:T(8,128)S(1)}, f32[256,256]{1,0:T(8,128)S(1)}) custom-call(bf16[128,256]{1,0:T(8,128)(2,1)} %q_hbm.1, bf16[128,128]{1,0:T(8,128)(2,1)} %k_hbm.1, bf16[128,128]{1,0:T(8,128)(2,1)} %v_hbm.1, bf16[128,2048]{1,0:T(8,128)(2,1)} %hid_ref.1, f32[2,4,128]{2,1,0:T(4,128)} %bitcast.2, ...), custom_call_target="tpu_custom_call" | custom-call | tf_op jit(solution)/shard_map/pallas_call | solution.py:485
  24.8 0.8 %shard_map.121 = (f32[128,256]{1,0:T(8,128)}, f32[128,128]{1,0:T(8,128)}, f32[128,128]{1,0:T(8,128)}, f32[256,256]{1,0:T(8,128)}) custom-call(f32[128,256]{1,0:T(8,128)S(1)} %get-tuple-element.8.refs_0_, f32[128,128]{1,0:T(8,128)S(1)} %get-tuple-element.9.refs_1_, f32[128,128]{1,0:T(8,128)S(1)} %get-tuple-element.10.refs_2_, ...), custom_call_target="tpu_custom_call" | custom-call | tf_op jit(solution)/shard_map/pallas_call | solution.py:520
